TPU v7x, 32 devices: a whole 2x2x4 slice. The times are simulated.
32 devices in a mesh: grp: 1, ep: 32 (over z, y, x, core).
Axes of the slice: x: 2, y: 2, z: 4, core: 2. Of those that a mesh axis runs over, the one named last changes fastest.
Arguments:
- tokens: bfloat16 [64, 2048], P('grp', 'ep'), may hold values from -6 to 6
- w_query: bfloat16 [2048, 1024], P('ep'), may hold values from -0.125 to 0.125
- w_key: bfloat16 [2048, 1024], P('ep'), may hold values from -0.125 to 0.125
- w_value: bfloat16 [2048, 1024], P('ep'), may hold values from -0.125 to 0.125
- w_forget: bfloat16 [2048, 16], P('ep'), may hold values from -0.125 to 0.125
- forget_bias: float32 [16], replicated, may hold values from -1 to 2
- cache_keys: bfloat16 [64, 1024, 1024], P(('grp', 'ep'))
- cache_values: bfloat16 [64, 1024, 1024], P(('grp', 'ep')), may hold values from -6 to 6
- cache_gates: float32 [64, 1024, 16], P(('grp', 'ep')), as said below
- lengths: int32 [64], P(('grp', 'ep')), may hold values from 128 to 1024, as said below
- w_out: bfloat16 [1024, 2048], P('ep'), may hold values from -0.1875 to 0.1875
- norm_gain: bfloat16 [2048], replicated, may hold values from 0.099609375 to 1.8984375
- w_router: bfloat16 [2048, 4], replicated, may hold values from -0.125 to 0.125
- routes: int32 [64, 2], P('grp'), may hold values from 0 to 3, all different within a row
- dense_gate: bfloat16 [2048], replicated, may hold values from -0.25 to 0.25
- dense_w_gate: bfloat16 [2048, 8192], P(None, 'ep'), may hold values from -0.125 to 0.125
- dense_w_up: bfloat16 [2048, 8192], P(None, 'ep'), may hold values from -0.125 to 0.125
- dense_w_down: bfloat16 [8192, 2048], P('ep'), may hold values from -0.125 to 0.125
- expert_w_gate: bfloat16 [2048, 16384], P(None, 'ep'), may hold values from -0.125 to 0.125
- expert_w_up: bfloat16 [2048, 16384], P(None, 'ep'), may hold values from -0.125 to 0.125
- expert_w_down: bfloat16 [16384, 2048], P('ep'), may hold values from -0.1875 to 0.1875
- final_gain: bfloat16 [2048], P('ep'), may hold values from 0.099609375 to 1.8984375
Outputs:
- result: bfloat16 [64, 2048], P('grp', 'ep')
Inputs may be any that keep to these rules, and one draw needn't show every extreme that they name: `routes`: each row names 2 different experts; every expert is named by some row. `lengths`: the first sequence of each part holds 1024 positions. `cache_gates`: never rising along positions.
All inputs are finite; a program needn't handle non-finite values.
Results may differ from a plain program's by a relative error of at most 0.0085.
Values may be sent and summed in bfloat16 or wider, within the bound.
A program may use at most 128 MiB of HBM per device.

v0:
```python
import jax
import jax.numpy as jnp
from jax import lax
from jax.sharding import PartitionSpec as P

EXP_SPLIT = 8
norm_eps = 1e-05
residual_scale = 8.0**0.25


def norm_rows(values, weights):
    center = jnp.mean(values, axis=-1, keepdims=True)
    second = jnp.mean(values * values, axis=-1, keepdims=True)
    return (
        (values - center)
        * lax.rsqrt(second - center * center + norm_eps)
        * weights.astype(jnp.float32)
    )


def attend(
    query,
    new_key,
    new_value,
    forget_pre,
    forget_bias,
    cache_keys,
    cache_values,
    cache_gates,
    lengths,
):
    seqs_here, width = query.shape
    heads = cache_gates.shape[2]
    head_size = width // heads
    cache_len = cache_keys.shape[1]
    query = query.reshape(seqs_here, heads, head_size)
    new_key = new_key.reshape(seqs_here, heads, head_size)
    new_value = new_value.reshape(seqs_here, heads, head_size)
    keys_all = cache_keys.reshape(seqs_here, cache_len, heads, head_size)
    values_all = cache_values.reshape(seqs_here, cache_len, heads, head_size)
    log_gate = jax.nn.log_sigmoid(forget_pre + forget_bias[None, :])
    position = jnp.arange(cache_len, dtype=jnp.int32)
    is_last = (position[None, :] == (lengths - 1)[:, None]).astype(jnp.float32)
    last_gate = jnp.sum(cache_gates * is_last[:, :, None], axis=1)
    bias = (last_gate + log_gate)[:, :, None] - jnp.transpose(cache_gates, (0, 2, 1))
    scale = head_size ** (-0.5)
    scores = (
        jnp.einsum("shd,slhd->shl", query, keys_all, preferred_element_type=jnp.float32) * scale
        + bias
    )
    valid = (position[None, :] < lengths[:, None])[:, None, :]
    scores = jnp.where(valid, scores, -jnp.inf)
    own_score = jnp.sum(query.astype(jnp.float32) * new_key.astype(jnp.float32), axis=-1) * scale
    top = jnp.maximum(jnp.max(scores, axis=-1), own_score)
    weights_cache = jnp.exp(scores - top[:, :, None])
    weight_own = jnp.exp(own_score - top)
    total = jnp.sum(weights_cache, axis=-1) + weight_own
    probs = (weights_cache / total[:, :, None]).astype(jnp.bfloat16)
    prob_own = (weight_own / total).astype(jnp.bfloat16)
    mixed = jnp.einsum("shl,slhd->shd", probs, values_all, preferred_element_type=jnp.float32)
    mixed = mixed + prob_own.astype(jnp.float32)[:, :, None] * new_value.astype(jnp.float32)
    return mixed.astype(jnp.bfloat16).reshape(seqs_here, width)


def shards(
    tokens,
    w_query,
    w_key,
    w_value,
    w_forget,
    forget_bias,
    cache_keys,
    cache_values,
    cache_gates,
    lengths,
    w_out,
    norm_gain,
    w_router,
    routes,
    dense_gate,
    dense_w_gate,
    dense_w_up,
    dense_w_down,
    expert_w_gate,
    expert_w_up,
    expert_w_down,
    final_gain,
):
    rank = lax.axis_index("ep")
    seqs_all, feat_dev = tokens.shape
    offset = rank * feat_dev
    terms = (
        jnp.dot(tokens, w_query, preferred_element_type=jnp.float32),
        jnp.dot(tokens, w_key, preferred_element_type=jnp.float32),
        jnp.dot(tokens, w_value, preferred_element_type=jnp.float32),
        jnp.dot(tokens, w_forget, preferred_element_type=jnp.float32),
    )
    query_sum, key_sum, value_sum, forget_pre = (
        lax.psum_scatter(terms[0], "ep", scatter_dimension=0, tiled=True),
        lax.psum_scatter(terms[1], "ep", scatter_dimension=0, tiled=True),
        lax.psum_scatter(terms[2], "ep", scatter_dimension=0, tiled=True),
        lax.psum_scatter(terms[3], "ep", scatter_dimension=0, tiled=True),
    )
    attn = attend(
        query_sum.astype(jnp.bfloat16),
        key_sum.astype(jnp.bfloat16),
        value_sum.astype(jnp.bfloat16),
        forget_pre,
        forget_bias,
        cache_keys,
        cache_values,
        cache_gates,
        lengths,
    )
    head_cols = lax.all_to_all(attn, "ep", split_axis=1, concat_axis=0, tiled=True)
    partial_sum = jnp.dot(head_cols, w_out, preferred_element_type=jnp.float32)
    residual = residual_scale * tokens.astype(jnp.float32)
    placed = lax.dynamic_slice_in_dim(partial_sum, offset, feat_dev, 1) + residual
    mixed = lax.psum(lax.dynamic_update_slice_in_dim(partial_sum, placed, offset, 1), "ep")
    normed = norm_rows(mixed, norm_gain).astype(jnp.bfloat16)
    logits = jnp.dot(normed, w_router, preferred_element_type=jnp.float32)
    expert_count = w_router.shape[1]
    picks = (routes[:, :, None] == jnp.arange(expert_count, dtype=jnp.int32)[None, None, :]).astype(
        jnp.float32
    )
    chosen = jnp.sum(logits[:, None, :] * picks, axis=-1)
    route_weight = jax.nn.softmax(chosen, axis=-1)
    expert_id = rank // EXP_SPLIT
    mine = jnp.sum(route_weight * (routes == expert_id).astype(jnp.float32), axis=1)
    expert_gate_part = jnp.dot(normed, expert_w_gate, preferred_element_type=jnp.float32)
    expert_up_part = jnp.dot(normed, expert_w_up, preferred_element_type=jnp.float32)
    expert_hidden = (mine[:, None] * jax.nn.silu(expert_gate_part) * expert_up_part).astype(
        jnp.bfloat16
    )
    dense_scale = jax.nn.sigmoid(jnp.dot(normed, dense_gate, preferred_element_type=jnp.float32))
    dense_gate_part = jnp.dot(normed, dense_w_gate, preferred_element_type=jnp.float32)
    dense_up_part = jnp.dot(normed, dense_w_up, preferred_element_type=jnp.float32)
    dense_hidden = (dense_scale[:, None] * jax.nn.silu(dense_gate_part) * dense_up_part).astype(
        jnp.bfloat16
    )
    local_branch = jnp.dot(
        expert_hidden, expert_w_down, preferred_element_type=jnp.float32
    ) + jnp.dot(dense_hidden, dense_w_down, preferred_element_type=jnp.float32)
    branch = lax.psum(local_branch, "ep")
    final = residual_scale * normed.astype(jnp.float32) + branch
    center = jnp.mean(final, axis=-1, keepdims=True)
    second = jnp.mean(final * final, axis=-1, keepdims=True)
    unit = (final - center) * lax.rsqrt(second - center * center + norm_eps)
    result = (
        lax.dynamic_slice_in_dim(unit, offset, feat_dev, 1)
        * final_gain.astype(jnp.float32)[None, :]
    )
    return result.astype(jnp.bfloat16)


def solution(mesh):
    placed = (
        P("grp", "ep"),
        P("ep", None),
        P("ep", None),
        P("ep", None),
        P("ep", None),
        P(),
        P(("grp", "ep"), None, None),
        P(("grp", "ep"), None, None),
        P(("grp", "ep"), None, None),
        P(("grp", "ep")),
        P("ep", None),
        P(),
        P(),
        P("grp", None),
        P(),
        P(None, "ep"),
        P(None, "ep"),
        P("ep", None),
        P(None, "ep"),
        P(None, "ep"),
        P("ep", None),
        P("ep"),
    )
    return jax.shard_map(
        shards, mesh=mesh, in_specs=placed, out_specs=P("grp", "ep"), check_vma=False
    )
```

profile of v0, /device:TPU:0, one launch (start us, length us, event | category | flops | bytes accessed | tf_op | source)
XLA Modules:
  0.0 374.7 jit_solution(17475962631380918628)
XLA Ops:
  6.5 0.0 copy-start
  6.5 0.8 broadcast_add_fusion
  7.3 0.7 iota_compare_fusion
  8.1 0.8 fusion.49
  8.9 1.1 fusion.47
  10.0 1.1 fusion.50
  11.1 1.1 fusion.51
  12.2 52.3 %all-reduce.12 = (bf16[64,1024]{1,0:T(8,128)(2,1)S(1)}, f32[64,16]{1,0:T(8,128)S(1)}, bf16[64,1024]{1,0:T(8,128)(2,1)S(1)}, bf16[64,1024]{1,0:T(8,128)(2,1)S(1)}) all-reduce(f32[64,1024]{1,0:T(8,128)S(1)} %fusion.47, f32[64,16]{1,0:T(8,128)S(1)} %fusion.49, f32[64,1024]{1,0:T(8,128)S(1)} %fusion.50, ...), channel_id=2, replica_groups=mesh['grp'=1,'ep'=32] {'ep'}, use_global_device_ids=true, to_apply=%region_0.0.clone | all-reduce | flops 197632 | bytes 1187840
  64.5 0.1 reshape.129
  64.6 0.1 reshape.141
  64.7 0.1 compare_convert_fusion
  64.8 0.1 reshape.133
  64.9 0.1 reshape.132
  65.0 0.0 copy-start.3
  65.0 6.2 %copy.39 = bf16[2,1024,1024]{1,2,0:T(8,128)(2,1)} copy(bf16[2,1024,1024]{2,1,0:T(8,128)(2,1)} %param.28) | data formatting | bytes 8388608 | tf_op args[6]
  71.2 0.0 copy-done.3
  71.2 0.1 multiply_reduce_fusion.2
  71.3 0.1 multiply_reduce_fusion.3
  71.4 0.0 copy-start.10
  71.4 2.9 fusion.48
  74.3 0.0 copy-done.10
  74.3 0.2 fusion.45
  74.5 0.2 fusion.16
  74.7 0.1 fusion.25
  74.8 6.2 %copy.40 = bf16[2,1024,1024]{1,2,0:T(8,128)(2,1)} copy(bf16[2,1024,1024]{2,1,0:T(8,128)(2,1)} %param.29) | data formatting | bytes 8388608 | tf_op args[7]
  81.0 0.0 copy-start.4
  81.0 3.4 fusion.8
  84.4 0.1 add_convert_fusion
  84.5 0.1 all_to_all.14
  84.6 0.6 copy.41
  85.2 3.4 all-to-all-start
  88.6 0.0 all-reduce.9.cloned.1.call-start
  88.7 7.0 %all-to-all-done = bf16[2,32,32]{2,0,1:T(2,128)(2,1)S(1)} async-done(((bf16[2,32,32]{2,0,1:T(2,128)(2,1)}), bf16[2,32,32]{2,0,1:T(2,128)(2,1)S(1)}, u32[]{:S(2)}, u32[]{:S(2)}) %all-to-all-start) | async-done | bytes 4128 | tf_op jit(solution)/shard_map/all_to_all | solution.py:115
  95.8 0.0 copy-done.5
  95.8 0.2 fusion.52
  96.0 0.0 copy-done.4
  96.0 0.1 multiply_add_fusion.1
  96.1 0.4 dynamic_update_slice.3
  96.5 0.0 copy-start.2
  96.5 0.8 copy-done.2
  97.3 0.0 all-reduce.9.cloned.1.call-update
  97.3 0.0 all-reduce.11.cloned.1.call-start
  97.4 0.0 copy-done.7
  97.4 0.0 copy-done.8
  97.4 127.8 %all-reduce.9.cloned.1.call-done = f32[64,2048]{1,0:T(8,128)} async-done(((f32[64,2048]{1,0:T(8,128)}), f32[64,2048]{1,0:T(8,128)}) %all-reduce.9.cloned.1.call-update) | async-done | bytes 524304 | tf_op jit(solution)/shard_map/psum | solution.py:119
  225.2 1.2 fusion.44
  226.4 1.2 multiply_convert_fusion
  227.6 0.2 fusion.6
  227.8 0.0 copy-done.6
  227.8 0.2 fusion.53
  228.0 0.0 copy-done.9
  228.1 1.5 fusion.55
  229.6 2.1 fusion.54
  231.7 0.0 copy-done
  231.7 2.5 fusion.1
  234.2 0.0 copy-start.11
  234.2 0.0 copy-start.1
  234.2 3.2 convolution_add_fusion
  237.4 0.0 all-reduce.11.cloned.1.call-update
  237.5 0.0 copy-done.11
  237.5 128.2 %all-reduce.11.cloned.1.call-done = f32[64,2048]{1,0:T(8,128)} async-done(((f32[64,2048]{1,0:T(8,128)}), f32[64,2048]{1,0:T(8,128)}) %all-reduce.11.cloned.1.call-update) | async-done | bytes 524304 | tf_op jit(solution)/shard_map/psum | solution.py:144
  365.7 0.0 copy-done.1
  365.7 1.4 fusion.43
  367.1 0.7 fusion.28
  (19 shorter events, 0.2 us)
Async XLA Ops:
  6.5 225.2 %copy-start = (bf16[512,2048]{1,0:T(8,128)(2,1)S(1)}, bf16[512,2048]{1,0:T(8,128)(2,1)}, u32[]{:S(2)}) copy-start(bf16[512,2048]{1,0:T(8,128)(2,1)} %param.42) | copy-start | bytes 6291460
  65.0 6.2 %copy-start.3 = (f32[2,1024,16]{1,2,0:T(8,128)S(1)}, f32[2,1024,16]{1,2,0:T(8,128)}, u32[]{:S(2)}) copy-start(f32[2,1024,16]{1,2,0:T(8,128)} %param.30) | copy-start | bytes 393220
  71.4 2.9 copy-start.10
  81.0 14.8 %copy-start.5 = (bf16[32,2048]{1,0:T(8,128)(2,1)S(1)}, bf16[32,2048]{1,0:T(8,128)(2,1)}, u32[]{:S(2)}) copy-start(bf16[32,2048]{1,0:T(8,128)(2,1)} %param.32) | copy-start | bytes 393220
  81.0 15.0 %copy-start.4 = (bf16[64,64]{1,0:T(8,128)(2,1)S(1)}, bf16[64,64]{1,0:T(8,128)(2,1)}, u32[]{:S(2)}) copy-start(bf16[64,64]{1,0:T(8,128)(2,1)} %param.22) | copy-start | bytes 24580
  81.0 16.4 %copy-start.7 = (bf16[2048]{0:T(1024)(128)(2,1)S(1)}, bf16[2048]{0:T(1024)(128)(2,1)}, u32[]{:S(2)}) copy-start(bf16[2048]{0:T(1024)(128)(2,1)} %param.33) | copy-start | bytes 12292
  81.0 16.4 %copy-start.8 = (bf16[2048]{0:T(1024)(128)(2,1)S(1)}, bf16[2048]{0:T(1024)(128)(2,1)}, u32[]{:S(2)}) copy-start(bf16[2048]{0:T(1024)(128)(2,1)} %param.36) | copy-start | bytes 12292
  84.4 143.4 %copy-start.6 = (bf16[2048,4]{0,1:T(4,128)(2,1)S(1)}, bf16[2048,4]{0,1:T(4,128)(2,1)}, u32[]{:S(2)}) copy-start(bf16[2048,4]{0,1:T(4,128)(2,1)} %param.34) | copy-start | bytes 49156
  84.4 143.6 %copy-start.9 = (s32[64,2]{0,1:T(2,128)S(1)}, s32[64,2]{0,1:T(2,128)}, u32[]{:S(2)}) copy-start(s32[64,2]{0,1:T(2,128)} %param.35) | copy-start | bytes 1540
  85.2 10.5 %all-to-all-start = ((bf16[2,32,32]{2,0,1:T(2,128)(2,1)}), bf16[2,32,32]{2,0,1:T(2,128)(2,1)S(1)}, u32[]{:S(2)}, u32[]{:S(2)}) async-start(bf16[2,32,32]{2,0,1:T(2,128)(2,1)} %copy.41), calls=%async_computation | async-start | bytes 32768 | tf_op jit(solution)/shard_map/all_to_all | solution.py:115
  88.6 136.6 %all-reduce.9.cloned.1.call-start = ((), (), s32[]{:S(2)}) async-start(), calls=%async_computation.1 | async-start | bytes 1048576 | tf_op jit(solution)/shard_map/psum | solution.py:119
  96.5 0.8 copy-start.2
  97.3 268.4 %all-reduce.11.cloned.1.call-start = ((), (), s32[]{:S(2)}) async-start(), calls=%async_computation.2 | async-start | bytes 1048576 | tf_op jit(solution)/shard_map/psum | solution.py:144
  234.2 3.3 copy-start.11
  234.2 131.5 %copy-start.1 = (f32[64,2048]{1,0:T(8,128)S(1)}, f32[64,2048]{1,0:T(8,128)}, u32[]{:S(2)}) copy-start(f32[64,2048]{1,0:T(8,128)} %all-reduce.9.cloned.1.call-done) | copy-start | bytes 1572868
Sparse Core Ops, SparseCore 0:
  97.4 127.7 all-reduce.8
  237.6 128.0 all-reduce.10
where the time goes:
time: 375 us
  waiting for transfers between devices  263 us (70%)
  blocking collectives  52.3 us (14%)
  matrix products  20.2 us (5%)
  local copies, waits for them, and re-layouts  14.8 us (4%)
  between operations  13.7 us (4%)
  other arithmetic  7.07 us (2%)
    psum x1, waiting for transfers between devices, shards(): branch = lax.psum(local_branch, 'ep')  128 us
    psum x1, waiting for transfers between devices, shards(): lax.psum(lax.dynamic_update_slice_in_dim(partial_sum, placed, offset, 1),...  128 us
    unnamed x1, blocking collectives  52.3 us
    unnamed x27, local copies, waits for them, and re-layouts  13.3 us
  transfers between devices with their start and end apart: 3, of which 3 were waited for; matrix products, arithmetic and copies ran while one was open for 0% of the time, Pallas kernels for 0%

commit v1 on v0

--- a/solution.py
+++ b/solution.py
@@ -141,7 +141,12 @@
     local_branch = jnp.dot(
         expert_hidden, expert_w_down, preferred_element_type=jnp.float32
     ) + jnp.dot(dense_hidden, dense_w_down, preferred_element_type=jnp.float32)
-    branch = lax.psum(local_branch, "ep")
+    n_blocks = lax.axis_size("ep")
+    branch = local_branch
+    for pp in [
+        [(jj, jj ^ kk) for jj in range(n_blocks)] for kk in (1, 2, 4, 8, 16) if kk < n_blocks
+    ]:
+        branch = branch + lax.ppermute(branch, "ep", pp)
     final = residual_scale * normed.astype(jnp.float32) + branch
     center = jnp.mean(final, axis=-1, keepdims=True)
     second = jnp.mean(final * final, axis=-1, keepdims=True)

time: 375 us -> 311 us (0.83)
  waiting for transfers between devices: 263 us -> 194 us
  starting transfers between devices: 3.51 us -> 9.67 us
    psum x1 -> x0, waiting for transfers between devices: 128 us -> none  [shards(): branch = lax.psum(local_branch, 'ep')]
    ppermute x0 -> x5, waiting for transfers between devices: none -> 58.9 us  [shards(): branch = branch + lax.ppermute(branch, 'ep', pp)]
    ppermute x0 -> x5, starting transfers between devices: none -> 6.2 us  [shards(): branch = branch + lax.ppermute(branch, 'ep', pp)]
  transfers between devices with their start and end apart: 3 -> 7, of which waited for: 3 -> 7; matrix products, arithmetic and copies ran while one was open for 0% -> 0% of each run, Pallas kernels for 0% -> 0%
where the time goes in v1:
time: 311 us; the launch traced here: 310 us
  waiting for transfers between devices  194 us (62%)
  blocking collectives  52.3 us (17%)
  matrix products  19.4 us (6%)
  local copies, waits for them, and re-layouts  14.8 us (5%)
  between operations  13.7 us (4%)
  starting transfers between devices  9.67 us (3%)
  other arithmetic  6.29 us (2%)
    psum x1, waiting for transfers between devices, shards(): lax.psum(lax.dynamic_update_slice_in_dim(partial_sum, placed, offset, 1),...  128 us
    ppermute x5, waiting for transfers between devices, shards(): branch = branch + lax.ppermute(branch, 'ep', pp)  58.9 us
    unnamed x1, blocking collectives  52.3 us
    unnamed x27, local copies, waits for them, and re-layouts  13.3 us
    all_to_all x1, waiting for transfers between devices, shards(): lax.all_to_all(attn, 'ep', split_axis=1, concat_axis=0, tiled=True)  7.05 us
  transfers between devices with their start and end apart: 7, of which 7 were waited for; matrix products, arithmetic and copies ran while one was open for 0% of the time, Pallas kernels for 0%

profile of v1, /device:TPU:0, one launch (start us, length us, event | category | flops | bytes accessed | tf_op | source)
XLA Modules:
  0.0 309.8 jit_solution(988514097004039675)
XLA Ops:
  6.5 0.0 copy-start
  6.5 0.8 broadcast_add_fusion
  7.3 0.7 iota_compare_fusion
  8.1 0.8 fusion.49
  8.9 1.1 fusion.47
  10.0 1.1 fusion.50
  11.1 1.1 fusion.51
  12.2 52.3 %all-reduce.9 = (bf16[64,1024]{1,0:T(8,128)(2,1)S(1)}, f32[64,16]{1,0:T(8,128)S(1)}, bf16[64,1024]{1,0:T(8,128)(2,1)S(1)}, bf16[64,1024]{1,0:T(8,128)(2,1)S(1)}) all-reduce(f32[64,1024]{1,0:T(8,128)S(1)} %fusion.47, f32[64,16]{1,0:T(8,128)S(1)} %fusion.49, f32[64,1024]{1,0:T(8,128)S(1)} %fusion.50, ...), channel_id=2, replica_groups=mesh['grp'=1,'ep'=32] {'ep'}, use_global_device_ids=true, to_apply=%region_0.0.clone | all-reduce | flops 197632 | bytes 1187840
  64.5 0.1 reshape.129
  64.6 0.1 reshape.141
  64.7 0.1 compare_convert_fusion
  64.8 0.1 reshape.133
  64.9 0.1 reshape.132
  64.9 6.2 %copy.39 = bf16[2,1024,1024]{1,2,0:T(8,128)(2,1)} copy(bf16[2,1024,1024]{2,1,0:T(8,128)(2,1)} %param.28) | data formatting | bytes 8388608 | tf_op args[6]
  71.2 0.1 multiply_reduce_fusion.2
  71.3 0.1 multiply_reduce_fusion.3
  71.4 2.9 fusion.48
  74.3 0.2 fusion.45
  74.5 0.2 fusion.16
  74.6 0.1 fusion.25
  74.8 6.2 %copy.40 = bf16[2,1024,1024]{1,2,0:T(8,128)(2,1)} copy(bf16[2,1024,1024]{2,1,0:T(8,128)(2,1)} %param.29) | data formatting | bytes 8388608 | tf_op args[7]
  81.0 3.4 %fusion.8 = f32[2,16,1,64]{3,2,1,0:T(1,128)S(1)} fusion(bf16[2,1024,16,64]{1,3,2,0:T(8,128)(2,1)} %bitcast.57, bf16[2,16,1024,1]{2,1,0,3:T(8,128)(2,1)S(1)} %fusion.25), kind=kOutput, calls=%fused_computation.18 | convolution fusion | flops 4194304 | bytes 4268032 | tf_op jit(solution)/shard_map/shl,slhd->shd/dot_general | solution.py:60
  84.4 0.1 add_convert_fusion
  84.5 0.1 all_to_all.14
  84.6 0.6 copy.41
  85.2 3.4 %all-to-all-start = ((bf16[2,32,32]{2,0,1:T(2,128)(2,1)}), bf16[2,32,32]{2,0,1:T(2,128)(2,1)S(1)}, u32[]{:S(2)}, u32[]{:S(2)}) async-start(bf16[2,32,32]{2,0,1:T(2,128)(2,1)} %copy.41), calls=%async_computation | async-start | bytes 32768 | tf_op jit(solution)/shard_map/all_to_all | solution.py:115
  88.6 0.0 all-reduce.8.cloned.1.call-start
  88.7 7.0 %all-to-all-done = bf16[2,32,32]{2,0,1:T(2,128)(2,1)S(1)} async-done(((bf16[2,32,32]{2,0,1:T(2,128)(2,1)}), bf16[2,32,32]{2,0,1:T(2,128)(2,1)S(1)}, u32[]{:S(2)}, u32[]{:S(2)}) %all-to-all-start) | async-done | bytes 4128 | tf_op jit(solution)/shard_map/all_to_all | solution.py:115
  95.7 0.0 copy-done.5
  95.7 0.2 fusion.52
  95.9 0.1 multiply_add_fusion
  96.0 0.4 dynamic_update_slice.3
  96.5 0.8 copy-done.2
  97.3 0.0 all-reduce.8.cloned.1.call-update
  97.3 0.0 copy-done.7
  97.4 127.8 %all-reduce.8.cloned.1.call-done = f32[64,2048]{1,0:T(8,128)} async-done(((f32[64,2048]{1,0:T(8,128)}), f32[64,2048]{1,0:T(8,128)}) %all-reduce.8.cloned.1.call-update) | async-done | bytes 524304 | tf_op jit(solution)/shard_map/psum | solution.py:119
  225.2 1.2 fusion.44
  226.4 1.2 multiply_convert_fusion
  227.6 0.2 fusion.6
  227.8 0.2 fusion.53
  228.0 0.0 copy-done.9
  228.0 1.5 fusion.55
  229.6 2.1 fusion.54
  231.7 0.0 copy-done
  231.7 2.5 fusion.1
  234.2 2.3 convolution_add_fusion
  236.5 0.1 collective-permute-start
  236.6 1.9 collective-permute-done
  238.5 0.1 add.114
  238.6 0.0 copy-start.11
  238.6 1.5 collective-permute-start.1
  240.2 12.5 %collective-permute-done.1 = f32[64,2048]{1,0:T(8,128)S(1)} collective-permute-done((f32[64,2048]{1,0:T(8,128)S(1)}, f32[64,2048]{1,0:T(8,128)S(1)}, u32[]{:S(2)}, u32[]{:S(2)}) %collective-permute-start.1) | collective-permute-done | bytes 524320 | tf_op jit(solution)/shard_map/ppermute | solution.py:149
  252.6 0.1 add.115
  252.7 1.5 collective-permute-start.2
  254.2 11.6 %collective-permute-done.2 = f32[64,2048]{1,0:T(8,128)S(1)} collective-permute-done((f32[64,2048]{1,0:T(8,128)S(1)}, f32[64,2048]{1,0:T(8,128)S(1)}, u32[]{:S(2)}, u32[]{:S(2)}) %collective-permute-start.2) | collective-permute-done | bytes 524320 | tf_op jit(solution)/shard_map/ppermute | solution.py:149
  265.9 0.1 add.116
  265.9 1.5 collective-permute-start.3
  267.5 10.8 %collective-permute-done.3 = f32[64,2048]{1,0:T(8,128)S(1)} collective-permute-done((f32[64,2048]{1,0:T(8,128)S(1)}, f32[64,2048]{1,0:T(8,128)S(1)}, u32[]{:S(2)}, u32[]{:S(2)}) %collective-permute-start.3) | collective-permute-done | bytes 524320 | tf_op jit(solution)/shard_map/ppermute | solution.py:149
  278.3 0.1 add.117
  278.3 1.5 collective-permute-start.4
  279.8 0.0 copy-done.11
  279.9 22.1 %collective-permute-done.4 = f32[64,2048]{1,0:T(8,128)S(1)} collective-permute-done((f32[64,2048]{1,0:T(8,128)S(1)}, f32[64,2048]{1,0:T(8,128)S(1)}, u32[]{:S(2)}, u32[]{:S(2)}) %collective-permute-start.4) | collective-permute-done | bytes 524320 | tf_op jit(solution)/shard_map/ppermute | solution.py:149
  301.9 0.3 fusion.43
  302.3 0.7 fusion.28
  (30 shorter events, 0.2 us)
Async XLA Ops:
  6.5 225.1 %copy-start = (bf16[512,2048]{1,0:T(8,128)(2,1)S(1)}, bf16[512,2048]{1,0:T(8,128)(2,1)}, u32[]{:S(2)}) copy-start(bf16[512,2048]{1,0:T(8,128)(2,1)} %param.42) | copy-start | bytes 6291460
  64.9 6.2 %copy-start.3 = (f32[2,1024,16]{1,2,0:T(8,128)S(1)}, f32[2,1024,16]{1,2,0:T(8,128)}, u32[]{:S(2)}) copy-start(f32[2,1024,16]{1,2,0:T(8,128)} %param.30) | copy-start | bytes 393220
  71.4 2.9 copy-start.10
  81.0 14.8 %copy-start.5 = (bf16[32,2048]{1,0:T(8,128)(2,1)S(1)}, bf16[32,2048]{1,0:T(8,128)(2,1)}, u32[]{:S(2)}) copy-start(bf16[32,2048]{1,0:T(8,128)(2,1)} %param.32) | copy-start | bytes 393220
  81.0 15.0 %copy-start.4 = (bf16[64,64]{1,0:T(8,128)(2,1)S(1)}, bf16[64,64]{1,0:T(8,128)(2,1)}, u32[]{:S(2)}) copy-start(bf16[64,64]{1,0:T(8,128)(2,1)} %param.22) | copy-start | bytes 24580
  81.0 16.3 %copy-start.7 = (bf16[2048]{0:T(1024)(128)(2,1)S(1)}, bf16[2048]{0:T(1024)(128)(2,1)}, u32[]{:S(2)}) copy-start(bf16[2048]{0:T(1024)(128)(2,1)} %param.33) | copy-start | bytes 12292
  81.0 16.4 %copy-start.8 = (bf16[2048]{0:T(1024)(128)(2,1)S(1)}, bf16[2048]{0:T(1024)(128)(2,1)}, u32[]{:S(2)}) copy-start(bf16[2048]{0:T(1024)(128)(2,1)} %param.36) | copy-start | bytes 12292
  84.4 143.4 %copy-start.6 = (bf16[2048,4]{0,1:T(4,128)(2,1)S(1)}, bf16[2048,4]{0,1:T(4,128)(2,1)}, u32[]{:S(2)}) copy-start(bf16[2048,4]{0,1:T(4,128)(2,1)} %param.34) | copy-start | bytes 49156
  84.4 143.6 %copy-start.9 = (s32[64,2]{0,1:T(2,128)S(1)}, s32[64,2]{0,1:T(2,128)}, u32[]{:S(2)}) copy-start(s32[64,2]{0,1:T(2,128)} %param.35) | copy-start | bytes 1540
  85.2 10.5 %all-to-all-start = ((bf16[2,32,32]{2,0,1:T(2,128)(2,1)}), bf16[2,32,32]{2,0,1:T(2,128)(2,1)S(1)}, u32[]{:S(2)}, u32[]{:S(2)}) async-start(bf16[2,32,32]{2,0,1:T(2,128)(2,1)} %copy.41), calls=%async_computation | async-start | bytes 32768 | tf_op jit(solution)/shard_map/all_to_all | solution.py:115
  88.6 136.6 %all-reduce.8.cloned.1.call-start = ((), (), s32[]{:S(2)}) async-start(), calls=%async_computation.1 | async-start | bytes 1048576 | tf_op jit(solution)/shard_map/psum | solution.py:119
  96.5 0.8 copy-start.2
  236.5 2.0 collective-permute-start
  238.6 41.3 %copy-start.11 = (bf16[64]{0:T(256)(128)(2,1)S(1)}, bf16[64]{0:T(256)(128)(2,1)}, u32[]{:S(2)}) copy-start(bf16[64]{0:T(256)(128)(2,1)} %param.43) | copy-start | bytes 388
  238.6 63.3 %copy-start.1 = (f32[64,2048]{1,0:T(8,128)S(1)}, f32[64,2048]{1,0:T(8,128)}, u32[]{:S(2)}) copy-start(f32[64,2048]{1,0:T(8,128)} %all-reduce.8.cloned.1.call-done) | copy-start | bytes 1572868
  238.6 14.0 %collective-permute-start.1 = (f32[64,2048]{1,0:T(8,128)S(1)}, f32[64,2048]{1,0:T(8,128)S(1)}, u32[]{:S(2)}, u32[]{:S(2)}) collective-permute-start(f32[64,2048]{1,0:T(8,128)S(1)} %add.114), channel_id=1, source_target_pairs={{0,2},{1,3},{2,0},{3,1},{4,6},{5,7},{6,4},{7,5},{8,10},{9,11},{10,... | collective-permute-start | bytes 1572872 | tf_op jit(solution)/shard_map/ppermute | solution.py:149
  252.7 13.2 %collective-permute-start.2 = (f32[64,2048]{1,0:T(8,128)S(1)}, f32[64,2048]{1,0:T(8,128)S(1)}, u32[]{:S(2)}, u32[]{:S(2)}) collective-permute-start(f32[64,2048]{1,0:T(8,128)S(1)} %add.115), channel_id=1, source_target_pairs={{0,4},{1,5},{2,6},{3,7},{4,0},{5,1},{6,2},{7,3},{8,12},{9,13},{10,... | collective-permute-start | bytes 1572872 | tf_op jit(solution)/shard_map/ppermute | solution.py:149
  265.9 12.3 %collective-permute-start.3 = (f32[64,2048]{1,0:T(8,128)S(1)}, f32[64,2048]{1,0:T(8,128)S(1)}, u32[]{:S(2)}, u32[]{:S(2)}) collective-permute-start(f32[64,2048]{1,0:T(8,128)S(1)} %add.116), channel_id=1, source_target_pairs={{0,8},{1,9},{2,10},{3,11},{4,12},{5,13},{6,14},{7,15},{8,0},{9,1},... | collective-permute-start | bytes 1572872 | tf_op jit(solution)/shard_map/ppermute | solution.py:149
  278.3 23.6 %collective-permute-start.4 = (f32[64,2048]{1,0:T(8,128)S(1)}, f32[64,2048]{1,0:T(8,128)S(1)}, u32[]{:S(2)}, u32[]{:S(2)}) collective-permute-start(f32[64,2048]{1,0:T(8,128)S(1)} %add.117), channel_id=1, source_target_pairs={{0,16},{1,17},{2,18},{3,19},{4,20},{5,21},{6,22},{7,23},{8,24},{9,... | collective-permute-start | bytes 1572872 | tf_op jit(solution)/shard_map/ppermute | solution.py:149
Sparse Core Ops, SparseCore 0:
  97.4 127.7 all-reduce.7
